TPU v7x, 32 devices: a whole 2x2x4 slice. The times are simulated.
32 devices in a mesh: gr: 2 (over x), fs: 8 (over z, y), tp: 2 (over core).
Axes of the slice: x: 2, y: 2, z: 4, core: 2. Of those that a mesh axis runs over, the one named last changes fastest.
Arguments:
- prompt: bfloat16 [3072, 2048], P(('gr', 'fs', 'tp')), may hold values from -6 to 6
- norm_first: float32 [2048], P(('gr', 'fs')), may hold values from 0.1 to 1.9
- gate_first: float32 [2048, 5632], P(('gr', 'fs'), 'tp'), may hold values from -6 to 6
- up_first: float32 [2048, 5632], P(('gr', 'fs'), 'tp'), may hold values from -6 to 6
- down_first: float32 [2048, 5632], P(('gr', 'fs'), 'tp'), may hold values from -6 to 6
- norm_second: float32 [2048], P(('gr', 'fs')), may hold values from 0.1 to 1.9
- gate_second: float32 [2048, 5632], P(('gr', 'fs'), 'tp'), may hold values from -6 to 6
- up_second: float32 [2048, 5632], P(('gr', 'fs'), 'tp'), may hold values from -6 to 6
- down_second: float32 [2048, 5632], P(('gr', 'fs'), 'tp'), may hold values from -6 to 6
Outputs:
- served_gate_first: bfloat16 [2048, 5632], P(None, 'fs')
- served_up_first: bfloat16 [2048, 5632], P(None, 'fs')
- served_down_first: bfloat16 [2048, 5632], P(None, 'fs')
- served_gate_second: bfloat16 [2048, 5632], P(None, 'fs')
- served_up_second: bfloat16 [2048, 5632], P(None, 'fs')
- served_down_second: bfloat16 [2048, 5632], P(None, 'fs')
- result: bfloat16 [3072, 2048], P(('gr', 'fs', 'tp'))
All inputs are finite; a program needn't handle non-finite values.
Results may differ from a plain program's by a relative error of at most 0.015.
Values may be sent and summed in bfloat16 or wider, within the bound.
A program may use at most 128 MiB of HBM per device.

v0:
```python
import jax
import jax.numpy as jnp
from jax import lax
from jax.sharding import PartitionSpec as P

D = 2048
FF = 5632
EPS = 1e-06


def fold_rows(gain, weight):
    return (gain[:, None] * weight).astype(jnp.bfloat16)


def relayout(stacked):
    moved = lax.all_to_all(
        lax.all_to_all(stacked, "tp", split_axis=1, concat_axis=2, tiled=True),
        "fs",
        split_axis=2,
        concat_axis=1,
        tiled=True,
    )
    whole = lax.all_gather(moved, ("gr", "tp"), axis=1, tiled=True)
    matrices = stacked.shape[0]
    block_width = moved.shape[2]
    gr_size = lax.axis_size("gr")
    tp_size = lax.axis_size("tp")
    fs_size = lax.axis_size("fs")
    sub_rows = stacked.shape[1] // tp_size
    shaped = whole.reshape(matrices, gr_size, tp_size, fs_size, sub_rows, block_width)
    return shaped.transpose(0, 1, 3, 2, 4, 5).reshape(
        matrices, gr_size * fs_size * tp_size * sub_rows, block_width
    )


def half_step(residual, weights):
    gate_weight = weights[0]
    up_weight = weights[1]
    down_weight = weights[2]
    resid_f = residual.astype(jnp.float32)
    normed = (
        resid_f * lax.rsqrt(jnp.mean(resid_f * resid_f, axis=-1, keepdims=True) + EPS)
    ).astype(jnp.bfloat16)
    in_scale = D ** (-0.5)
    out_scale = FF ** (-0.5)
    tokens_in = lax.all_gather(normed, "fs", axis=0, tiled=True)
    gate_pre = jnp.dot(tokens_in, gate_weight, preferred_element_type=jnp.float32) * in_scale
    up_pre = jnp.dot(tokens_in, up_weight, preferred_element_type=jnp.float32) * in_scale
    hidden = (jax.nn.silu(gate_pre) * up_pre).astype(jnp.bfloat16)
    branch = lax.psum_scatter(
        (
            lax.dot_general(
                hidden, down_weight, (((1,), (1,)), ((), ())), preferred_element_type=jnp.float32
            )
            * out_scale
        ).astype(jnp.bfloat16),
        "fs",
        scatter_dimension=0,
        tiled=True,
    ).astype(jnp.float32)
    return (resid_f + 0.5 * branch).astype(jnp.bfloat16)


def on_device(
    prompt,
    norm_first,
    gate_first,
    up_first,
    down_first,
    norm_second,
    gate_second,
    up_second,
    down_second,
):
    first_set = jnp.stack(
        [
            fold_rows(norm_first, gate_first),
            fold_rows(norm_first, up_first),
            down_first.astype(jnp.bfloat16),
        ]
    )
    second_set = jnp.stack(
        [
            fold_rows(norm_second, gate_second),
            fold_rows(norm_second, up_second),
            down_second.astype(jnp.bfloat16),
        ]
    )
    served_first = relayout(first_set)
    middle = half_step(prompt, served_first)
    served_second = relayout(second_set)
    result = half_step(middle, served_second)
    return (
        served_first[0],
        served_first[1],
        served_first[2],
        served_second[0],
        served_second[1],
        served_second[2],
        result,
    )


def solution(mesh):
    in_specs = (
        P(("gr", "fs", "tp"), None),
        P(("gr", "fs")),
        P(("gr", "fs"), "tp"),
        P(("gr", "fs"), "tp"),
        P(("gr", "fs"), "tp"),
        P(("gr", "fs")),
        P(("gr", "fs"), "tp"),
        P(("gr", "fs"), "tp"),
        P(("gr", "fs"), "tp"),
    )
    out_specs = (
        P(None, "fs"),
        P(None, "fs"),
        P(None, "fs"),
        P(None, "fs"),
        P(None, "fs"),
        P(None, "fs"),
        P(("gr", "fs", "tp"), None),
    )
    return jax.shard_map(
        on_device, mesh=mesh, in_specs=in_specs, out_specs=out_specs, check_vma=False
    )
```

profile of v0, /device:TPU:0, one launch (start us, length us, event | category | flops | bytes accessed | tf_op | source)
XLA Modules:
  0.0 607.6 jit_solution(7273351563624397723)
XLA Ops:
  7.2 2.5 fusion.6
  9.7 0.2 pad_maximum_fusion
  10.0 1.9 copy.52
  11.8 6.0 all_to_all.72
  17.9 2.6 copy.77
  20.5 10.8 %copy.72 = bf16[3,64,2,2816]{1,0,3,2:T(4,128)(2,1)} copy(bf16[3,64,2,2816]{3,2,1,0:T(2,128)(2,1)S(1)} %bitcast.78) | data formatting | bytes 4325376 | tf_op jit(solution)/shard_map/all_to_all | solution.py:17
  31.3 7.1 %reshape.54 = bf16[8,2,67584]{2,1,0:T(2,128)(2,1)S(1)} reshape(bf16[5632,3,64]{2,1,0:T(4,128)(2,1)} %bitcast.56) | data formatting | bytes 4325376
  38.4 57.7 %all_to_all.73 = bf16[8,2,67584]{2,1,0:T(2,128)(2,1)} all-to-all(bf16[8,2,67584]{2,1,0:T(2,128)(2,1)S(1)} %reshape.54), channel_id=1, replica_groups=mesh['gr'=2,'fs'=8,'tp'=2] {'fs'}, dimensions={0} | all-to-all | bytes 4325376 | tf_op jit(solution)/shard_map/all_to_all | solution.py:16
  96.1 8.0 %reshape.55 = bf16[5632,3,64]{2,1,0:T(4,128)(2,1)} reshape(bf16[8,2,67584]{2,1,0:T(2,128)(2,1)} %all_to_all.73) | data formatting | bytes 4325376
  104.1 9.4 %copy.55 = bf16[3,64,8,704]{3,1,2,0:T(8,128)(2,1)} copy(bf16[3,64,8,704]{1,0,3,2:T(4,128)(2,1)} %bitcast.57) | data formatting | bytes 4325376 | tf_op jit(solution)/shard_map/all_to_all | solution.py:16
  113.8 0.9 fusion.1
  114.7 0.3 reduce-scatter.3.cloned.1.call-start
  115.0 61.3 %all-gather.5.cloned.1.call-done = bf16[3,2048,704]{2,1,0:T(8,128)(2,1)} async-done(((bf16[3,512,704]{2,1,0:T(8,128)(2,1)}), bf16[3,2048,704]{2,1,0:T(8,128)(2,1)}) %all-gather.5.cloned.1.call-update) | async-done | bytes 8650768 | tf_op jit(solution)/shard_map/all_gather | solution.py:23
  176.3 4.1 fusion.15
  180.4 0.3 copy.56
  180.8 1.9 copy.57
  182.6 1.8 copy.58
  184.5 54.6 %all-gather.9.cloned.1.call-done = bf16[768,2048]{1,0:T(8,128)(2,1)} async-done(((bf16[96,2048]{1,0:T(8,128)(2,1)}), bf16[768,2048]{1,0:T(8,128)(2,1)}) %all-gather.9.cloned.1.call-update) | async-done | bytes 3145744 | tf_op jit(solution)/shard_map/all_gather | solution.py:46
  239.1 5.7 fusion.16
  244.8 12.4 %multiply_convert_fusion.1 = bf16[768,2048]{1,0:T(8,128)(2,1)} fusion(bf16[2048,704]{1,0:T(8,128)(2,1)} %bitcast.64, f32[768,704]{0,1:T(8,128)} %fusion.16, bf16[768,2048]{1,0:T(8,128)(2,1)} %all-gather.9.cloned.1.call-done, bf16[2048,704]{1,0:T(8,128)(2,1)} %bitcast.62), kind=kOutput, calls=%fused_computation.1 | convolution fusion | flops 4436656128 | bytes 14221312 | tf_op jit(solution)/shard_map/dot_general | solution.py:52
  257.3 0.5 all-gather.7.cloned.1.call-start
  257.9 2.5 fusion.8
  260.6 1.9 copy.59
  262.5 6.0 all_to_all.74
  268.5 3.9 copy.76
  272.5 15.1 %copy.73 = bf16[3,64,2,2816]{1,0,3,2:T(4,128)(2,1)} copy(bf16[3,64,2,2816]{3,2,1,0:T(2,128)(2,1)} %bitcast.79) | data formatting | bytes 4325376 | tf_op jit(solution)/shard_map/all_to_all | solution.py:17
  287.6 8.2 %reshape.56 = bf16[8,2,67584]{2,1,0:T(2,128)(2,1)} reshape(bf16[5632,3,64]{2,1,0:T(4,128)(2,1)} %bitcast.58) | data formatting | bytes 4325376
  295.9 67.8 %all_to_all.75 = bf16[8,2,67584]{2,1,0:T(2,128)(2,1)} all-to-all(bf16[8,2,67584]{2,1,0:T(2,128)(2,1)} %reshape.56), channel_id=1, replica_groups=mesh['gr'=2,'fs'=8,'tp'=2] {'fs'}, dimensions={0} | all-to-all | bytes 4325376 | tf_op jit(solution)/shard_map/all_to_all | solution.py:16
  363.7 8.0 %reshape.57 = bf16[5632,3,64]{2,1,0:T(4,128)(2,1)} reshape(bf16[8,2,67584]{2,1,0:T(2,128)(2,1)} %all_to_all.75) | data formatting | bytes 4325376
  371.6 9.4 %copy.62 = bf16[3,64,8,704]{3,1,2,0:T(8,128)(2,1)} copy(bf16[3,64,8,704]{1,0,3,2:T(4,128)(2,1)} %bitcast.59) | data formatting | bytes 4325376 | tf_op jit(solution)/shard_map/all_to_all | solution.py:16
  381.1 1.3 fusion.3
  382.4 1.9 fusion.4
  384.5 59.3 %all-gather.7.cloned.1.call-done = bf16[3,2048,704]{2,1,0:T(8,128)(2,1)} async-done(((bf16[3,512,704]{2,1,0:T(8,128)(2,1)}), bf16[3,2048,704]{2,1,0:T(8,128)(2,1)}) %all-gather.7.cloned.1.call-update) | async-done | bytes 8650768 | tf_op jit(solution)/shard_map/all_gather | solution.py:23
  443.8 4.1 fusion.14
  447.9 1.9 copy.63
  449.8 1.9 copy.64
  451.7 1.9 copy.65
  453.6 52.8 %all-gather.11.cloned.1.call-done = bf16[768,2048]{1,0:T(8,128)(2,1)} async-done(((bf16[96,2048]{1,0:T(8,128)(2,1)}), bf16[768,2048]{1,0:T(8,128)(2,1)}) %all-gather.11.cloned.1.call-update) | async-done | bytes 3145744 | tf_op jit(solution)/shard_map/all_gather | solution.py:46
  506.5 6.6 %fusion.17 = f32[768,704]{0,1:T(8,128)} fusion(bf16[768,2048]{1,0:T(8,128)(2,1)} %all-gather.11.cloned.1.call-done, bf16[2048,704]{1,0:T(8,128)(2,1)} %bitcast.66), kind=kOutput, calls=%fused_computation.39 | convolution fusion | flops 2214592512 | bytes 8192000 | tf_op jit(solution)/shard_map/dot_general | solution.py:47
  513.1 12.4 %multiply_convert_fusion = bf16[768,2048]{1,0:T(8,128)(2,1)} fusion(bf16[2048,704]{1,0:T(8,128)(2,1)} %bitcast.70, f32[768,704]{0,1:T(8,128)} %fusion.17, bf16[768,2048]{1,0:T(8,128)(2,1)} %all-gather.11.cloned.1.call-done, bf16[2048,704]{1,0:T(8,128)(2,1)} %bitcast.68), kind=kOutput, calls=%fused_computation | convolution fusion | flops 4436656128 | bytes 14221312 | tf_op jit(solution)/shard_map/dot_general | solution.py:52
  525.6 4.6 copy.69
  530.1 4.6 copy.70
  534.7 4.6 copy.71
  539.2 2.7 copy.66
  541.9 4.7 copy.67
  546.7 2.7 copy.68
  549.3 49.1 %reduce-scatter.5.cloned.1.call-done = bf16[96,2048]{1,0:T(8,128)(2,1)} async-done(((bf16[768,2048]{1,0:T(8,128)(2,1)}), bf16[96,2048]{1,0:T(8,128)(2,1)}) %reduce-scatter.5.cloned.1.call-update) | async-done | bytes 393232 | tf_op jit(solution)/shard_map/reduce_scatter | solution.py:50
  598.5 2.1 fusion.5
  (21 shorter events, 1.0 us)
Async XLA Ops:
  7.2 169.1 %all-gather.5.cloned.1.call-start = ((), (), s32[]{:S(2)}) async-start(), calls=%async_computation.6 | async-start | bytes 11796480 | tf_op jit(solution)/shard_map/all_gather | solution.py:23
  104.1 9.5 %copy-start.1 = (bf16[96,2048]{1,0:T(8,128)(2,1)S(1)}, bf16[96,2048]{1,0:T(8,128)(2,1)}, u32[]{:S(2)}) copy-start(bf16[96,2048]{1,0:T(8,128)(2,1)} %param.9) | copy-start | bytes 1179652
  113.5 125.6 %all-gather.9.cloned.1.call-start = ((), (), s32[]{:S(2)}) async-start(), calls=%async_computation.8 | async-start | bytes 3538944 | tf_op jit(solution)/shard_map/all_gather | solution.py:46
  114.7 266.4 %reduce-scatter.3.cloned.1.call-start = ((), (), s32[]{:S(2)}) async-start(), calls=%async_computation.9 | async-start | bytes 3538944 | tf_op jit(solution)/shard_map/reduce_scatter | solution.py:50
  257.2 0.7 copy-start.2
  257.3 186.5 %all-gather.7.cloned.1.call-start = ((), (), s32[]{:S(2)}) async-start(), calls=%async_computation.7 | async-start | bytes 11796480 | tf_op jit(solution)/shard_map/all_gather | solution.py:23
  381.0 125.4 %all-gather.11.cloned.1.call-start = ((), (), s32[]{:S(2)}) async-start(), calls=%async_computation.10 | async-start | bytes 3538944 | tf_op jit(solution)/shard_map/all_gather | solution.py:46
  384.3 214.2 %reduce-scatter.5.cloned.1.call-start = ((), (), s32[]{:S(2)}) async-start(), calls=%async_computation.11 | async-start | bytes 3538944 | tf_op jit(solution)/shard_map/reduce_scatter | solution.py:50
  541.9 4.7 copy-start
Sparse Core Ops, SparseCore 0:
  113.6 62.6 all-gather.4
  179.1 60.0 all-gather.8
  257.4 96.6 reduce-scatter.2
  381.2 62.5 all-gather.6
  446.4 60.0 all-gather.10
  525.7 72.7 reduce-scatter.4
where the time goes:
time: 615 us; the launch traced here: 608 us
  waiting for transfers between devices  277 us (45%)
  blocking collectives  138 us (22%)
  local copies, waits for them, and re-layouts  128 us (21%)
  matrix products  37.2 us (6%)
  between operations  14.4 us (2%)
  other arithmetic  11.8 us (2%)
    all_to_all x2, blocking collectives, relayout(): lax.all_to_all(lax.all_to_all(stacked, 'tp', split_axis=1, concat_axis=2,...  126 us
    all_gather x2, waiting for transfers between devices, relayout(): whole = lax.all_gather(moved, ('gr', 'tp'), axis=1, tiled=True)  121 us
    all_gather x2, waiting for transfers between devices, half_step(): tokens_in = lax.all_gather(normed, 'fs', axis=0, tiled=True)  107 us
    unnamed x16, local copies, waits for them, and re-layouts  55.2 us
    reduce_scatter x2, waiting for transfers between devices, half_step(): lax.psum_scatter((lax.dot_general(hidden, down_weight, (((1,), (1,)), (()...  49.1 us
    all_to_all x4, local copies, waits for them, and re-layouts, relayout(): lax.all_to_all(stacked, 'tp', split_axis=1, concat_axis=2, tiled=True)  32.4 us
    dot_general x2, matrix products, half_step(): lax.dot_general(hidden, down_weight, (((1,), (1,)), ((), ())), preferred_...  24.9 us
    all_to_all x2, local copies, waits for them, and re-layouts, relayout(): lax.all_to_all(lax.all_to_all(stacked, 'tp', split_axis=1, concat_axis=2,...  18.8 us
  transfers between devices with their start and end apart: 6, of which 5 were waited for; matrix products, arithmetic and copies ran while one was open for 16% of the time, Pallas kernels for 0%

commit v1 on v0

--- a/solution.py
+++ b/solution.py
@@ -6,6 +6,22 @@
 D = 2048
 FF = 5632
 EPS = 1e-06
+
+
+def bring_the_heaps(x_part):
+    store = []
+    src_i = 0
+    size_here = lax.axis_size("fs")
+    while src_i < size_here:
+        store.append((src_i, (src_i + 1) % size_here))
+        src_i = src_i + 1
+    big = [None] * size_here
+    big[size_here - 1] = x_part
+    for i in range(size_here - 2, -1, -1):
+        big[i] = lax.ppermute(big[i + 1], "fs", store)
+    return jnp.roll(
+        jnp.concatenate(big, axis=0), (lax.axis_index("fs") + 1) * x_part.shape[0], axis=0
+    )
 
 
 def fold_rows(gain, weight):
@@ -43,7 +59,7 @@
     ).astype(jnp.bfloat16)
     in_scale = D ** (-0.5)
     out_scale = FF ** (-0.5)
-    tokens_in = lax.all_gather(normed, "fs", axis=0, tiled=True)
+    tokens_in = bring_the_heaps(normed)
     gate_pre = jnp.dot(tokens_in, gate_weight, preferred_element_type=jnp.float32) * in_scale
     up_pre = jnp.dot(tokens_in, up_weight, preferred_element_type=jnp.float32) * in_scale
     hidden = (jax.nn.silu(gate_pre) * up_pre).astype(jnp.bfloat16)

time: 615 us -> 549 us (0.89)
  waiting for transfers between devices: 277 us -> 197 us
  local copies, waits for them, and re-layouts: 128 us -> 139 us
    ppermute x0 -> x14, waiting for transfers between devices: none -> 147 us  [bring_the_heaps(): big[i] = lax.ppermute(big[i + 1], 'fs', store)]
    all_gather x2, waiting for transfers between devices: 121 us -> 0.01 us  [relayout(): whole = lax.all_gather(moved, ('gr', 'tp'), axis=1, tiled=True)]
    all_gather x2 -> x0, waiting for transfers between devices: 107 us -> none  [half_step(): tokens_in = lax.all_gather(normed, 'fs', axis=0, tiled=True)]
    unnamed x16 -> x58, local copies, waits for them, and re-layouts: 55.2 us -> 67.6 us
  transfers between devices with their start and end apart: 6 -> 18, of which waited for: 5 -> 15; matrix products, arithmetic and copies ran while one was open for 16% -> 17% of each run, Pallas kernels for 0% -> 0%
where the time goes in v1:
time: 549 us; the launch traced here: 541 us
  waiting for transfers between devices  197 us (36%)
  local copies, waits for them, and re-layouts  139 us (25%)
  blocking collectives  138 us (25%)
  matrix products  38.4 us (7%)
  between operations  14.3 us (3%)
  other arithmetic  11.2 us (2%)
    ppermute x14, waiting for transfers between devices, bring_the_heaps(): big[i] = lax.ppermute(big[i + 1], 'fs', store)  147 us
    all_to_all x2, blocking collectives, relayout(): lax.all_to_all(lax.all_to_all(stacked, 'tp', split_axis=1, concat_axis=2,...  126 us
    unnamed x58, local copies, waits for them, and re-layouts  67.6 us
    reduce_scatter x2, waiting for transfers between devices, half_step(): lax.psum_scatter((lax.dot_general(hidden, down_weight, (((1,), (1,)), (()...  49.8 us
    all_to_all x4, local copies, waits for them, and re-layouts, relayout(): lax.all_to_all(stacked, 'tp', split_axis=1, concat_axis=2, tiled=True)  32.5 us
    dot_general x2, matrix products, half_step(): lax.dot_general(hidden, down_weight, (((1,), (1,)), ((), ())), preferred_...  26.7 us
    all_to_all x2, local copies, waits for them, and re-layouts, relayout(): lax.all_to_all(lax.all_to_all(stacked, 'tp', split_axis=1, concat_axis=2,...  18.8 us
    all_to_all x2, blocking collectives, relayout(): lax.all_to_all(stacked, 'tp', split_axis=1, concat_axis=2, tiled=True)  12.1 us
  transfers between devices with their start and end apart: 18, of which 15 were waited for; matrix products, arithmetic and copies ran while one was open for 17% of the time, Pallas kernels for 0%

profile of v1, /device:TPU:0, one launch (start us, length us, event | category | flops | bytes accessed | tf_op | source)
XLA Modules:
  0.0 540.6 jit_solution(12292680967409115006)
XLA Ops:
  7.2 2.5 fusion.8
  10.0 1.9 copy.52
  11.8 6.0 %all_to_all.72 = bf16[3,128,2816]{2,0,1:T(4,128)(2,1)S(1)} all-to-all(bf16[3,128,2816]{2,0,1:T(4,128)(2,1)S(1)} %copy.52), channel_id=1, replica_groups=mesh['gr'=2,'fs'=8,'tp'=2] {'tp'}, dimensions={1} | all-to-all | bytes 4325376 | tf_op jit(solution)/shard_map/all_to_all | solution.py:33
  17.9 2.6 copy.77
  20.5 10.8 %copy.72 = bf16[3,64,2,2816]{1,0,3,2:T(4,128)(2,1)} copy(bf16[3,64,2,2816]{3,2,1,0:T(2,128)(2,1)S(1)} %bitcast.74) | data formatting | bytes 4325376 | tf_op jit(solution)/shard_map/all_to_all | solution.py:33
  31.3 7.1 %reshape.54 = bf16[8,2,67584]{2,1,0:T(2,128)(2,1)S(1)} reshape(bf16[5632,3,64]{2,1,0:T(4,128)(2,1)} %bitcast.52) | data formatting | bytes 4325376
  38.4 57.7 %all_to_all.73 = bf16[8,2,67584]{2,1,0:T(2,128)(2,1)} all-to-all(bf16[8,2,67584]{2,1,0:T(2,128)(2,1)S(1)} %reshape.54), channel_id=1, replica_groups=mesh['gr'=2,'fs'=8,'tp'=2] {'fs'}, dimensions={0} | all-to-all | bytes 4325376 | tf_op jit(solution)/shard_map/all_to_all | solution.py:32
  96.2 7.9 %reshape.55 = bf16[5632,3,64]{2,1,0:T(4,128)(2,1)} reshape(bf16[8,2,67584]{2,1,0:T(2,128)(2,1)} %all_to_all.73) | data formatting | bytes 4325376
  104.1 9.4 %copy.55 = bf16[3,64,8,704]{3,1,2,0:T(8,128)(2,1)} copy(bf16[3,64,8,704]{1,0,3,2:T(4,128)(2,1)} %bitcast.53) | data formatting | bytes 4325376 | tf_op jit(solution)/shard_map/all_to_all | solution.py:32
  114.8 11.5 %collective-permute-done = bf16[96,2048]{1,0:T(8,128)(2,1)S(1)} collective-permute-done((bf16[96,2048]{1,0:T(8,128)(2,1)S(1)}, bf16[96,2048]{1,0:T(8,128)(2,1)S(1)}, u32[]{:S(2)}, u32[]{:S(2)}) %collective-permute-start) | collective-permute-done | bytes 393248 | tf_op jit(solution)/shard_map/ppermute | solution.py:21
  126.3 11.4 %collective-permute-done.1 = bf16[96,2048]{1,0:T(8,128)(2,1)S(1)} collective-permute-done((bf16[96,2048]{1,0:T(8,128)(2,1)S(1)}, bf16[96,2048]{1,0:T(8,128)(2,1)S(1)}, u32[]{:S(2)}, u32[]{:S(2)}) %collective-permute-start.1) | collective-permute-done | bytes 393248 | tf_op jit(solution)/shard_map/ppermute | solution.py:21
  137.7 10.6 %collective-permute-done.2 = bf16[96,2048]{1,0:T(8,128)(2,1)S(1)} collective-permute-done((bf16[96,2048]{1,0:T(8,128)(2,1)S(1)}, bf16[96,2048]{1,0:T(8,128)(2,1)S(1)}, u32[]{:S(2)}, u32[]{:S(2)}) %collective-permute-start.2) | collective-permute-done | bytes 393248 | tf_op jit(solution)/shard_map/ppermute | solution.py:21
  148.3 10.5 %collective-permute-done.3 = bf16[96,2048]{1,0:T(8,128)(2,1)S(1)} collective-permute-done((bf16[96,2048]{1,0:T(8,128)(2,1)S(1)}, bf16[96,2048]{1,0:T(8,128)(2,1)S(1)}, u32[]{:S(2)}, u32[]{:S(2)}) %collective-permute-start.3) | collective-permute-done | bytes 393248 | tf_op jit(solution)/shard_map/ppermute | solution.py:21
  158.7 11.5 %collective-permute-done.4 = bf16[96,2048]{1,0:T(8,128)(2,1)S(1)} collective-permute-done((bf16[96,2048]{1,0:T(8,128)(2,1)S(1)}, bf16[96,2048]{1,0:T(8,128)(2,1)S(1)}, u32[]{:S(2)}, u32[]{:S(2)}) %collective-permute-start.4) | collective-permute-done | bytes 393248 | tf_op jit(solution)/shard_map/ppermute | solution.py:21
  170.2 12.2 %collective-permute-done.5 = bf16[96,2048]{1,0:T(8,128)(2,1)S(1)} collective-permute-done((bf16[96,2048]{1,0:T(8,128)(2,1)S(1)}, bf16[96,2048]{1,0:T(8,128)(2,1)S(1)}, u32[]{:S(2)}, u32[]{:S(2)}) %collective-permute-start.5) | collective-permute-done | bytes 393248 | tf_op jit(solution)/shard_map/ppermute | solution.py:21
  182.9 10.4 %collective-permute-done.6 = bf16[96,2048]{1,0:T(8,128)(2,1)S(1)} collective-permute-done((bf16[96,2048]{1,0:T(8,128)(2,1)S(1)}, bf16[96,2048]{1,0:T(8,128)(2,1)S(1)}, u32[]{:S(2)}, u32[]{:S(2)}) %collective-permute-start.6) | collective-permute-done | bytes 393248 | tf_op jit(solution)/shard_map/ppermute | solution.py:21
  199.7 4.1 fusion.25
  204.1 1.9 copy.57
  207.9 6.6 %fusion.16 = f32[768,704]{0,1:T(8,128)} fusion(bf16[2048,704]{1,0:T(8,128)(2,1)S(1)} %bitcast.56, s32[]{:T(128)S(6)} %select_n.13, bf16[768,2048]{1,0:T(8,128)(2,1)} %constant_dynamic-update-slice_fusion), kind=kOutput, calls=%fused_computation.58 | convolution fusion | flops 2220883968 | bytes 8192004 | tf_op jit(solution)/shard_map/dot_general | solution.py:63
  214.4 13.3 %multiply_convert_fusion.1 = bf16[768,2048]{1,0:T(8,128)(2,1)} fusion(bf16[2048,704]{1,0:T(8,128)(2,1)} %bitcast.60, f32[768,704]{0,1:T(8,128)} %fusion.16, bf16[2048,704]{1,0:T(8,128)(2,1)} %bitcast.58, s32[]{:T(128)S(6)} %select_n.13, bf16[768,2048]{1,0:T(8,128)(2,1)} %constant_dynamic-update-slice_fusion), kind=kOutput, calls=%fused_computation.5 | convolution fusion | flops 4442947584 | bytes 14221316 | tf_op jit(solution)/shard_map/dot_general | solution.py:68
  228.4 2.5 fusion.10
  233.0 6.0 %all_to_all.74 = bf16[3,128,2816]{2,0,1:T(4,128)(2,1)S(1)} all-to-all(bf16[3,128,2816]{2,0,1:T(4,128)(2,1)S(1)} %copy.59), channel_id=1, replica_groups=mesh['gr'=2,'fs'=8,'tp'=2] {'tp'}, dimensions={1} | all-to-all | bytes 4325376 | tf_op jit(solution)/shard_map/all_to_all | solution.py:33
  239.1 3.9 copy.76
  243.0 15.1 %copy.73 = bf16[3,64,2,2816]{1,0,3,2:T(4,128)(2,1)} copy(bf16[3,64,2,2816]{3,2,1,0:T(2,128)(2,1)} %bitcast.75) | data formatting | bytes 4325376 | tf_op jit(solution)/shard_map/all_to_all | solution.py:33
  258.1 8.2 %reshape.56 = bf16[8,2,67584]{2,1,0:T(2,128)(2,1)} reshape(bf16[5632,3,64]{2,1,0:T(4,128)(2,1)} %bitcast.54) | data formatting | bytes 4325376
  266.4 67.8 %all_to_all.75 = bf16[8,2,67584]{2,1,0:T(2,128)(2,1)} all-to-all(bf16[8,2,67584]{2,1,0:T(2,128)(2,1)} %reshape.56), channel_id=1, replica_groups=mesh['gr'=2,'fs'=8,'tp'=2] {'fs'}, dimensions={0} | all-to-all | bytes 4325376 | tf_op jit(solution)/shard_map/all_to_all | solution.py:32
  334.2 7.9 %reshape.57 = bf16[5632,3,64]{2,1,0:T(4,128)(2,1)} reshape(bf16[8,2,67584]{2,1,0:T(2,128)(2,1)} %all_to_all.75) | data formatting | bytes 4325376
  342.1 9.4 %copy.62 = bf16[3,64,8,704]{3,1,2,0:T(8,128)(2,1)} copy(bf16[3,64,8,704]{1,0,3,2:T(4,128)(2,1)} %bitcast.55) | data formatting | bytes 4325376 | tf_op jit(solution)/shard_map/all_to_all | solution.py:32
  355.6 11.6 %collective-permute-done.7 = bf16[96,2048]{1,0:T(8,128)(2,1)S(1)} collective-permute-done((bf16[96,2048]{1,0:T(8,128)(2,1)S(1)}, bf16[96,2048]{1,0:T(8,128)(2,1)S(1)}, u32[]{:S(2)}, u32[]{:S(2)}) %collective-permute-start.7) | collective-permute-done | bytes 393248 | tf_op jit(solution)/shard_map/ppermute | solution.py:21
  368.0 11.6 %collective-permute-done.8 = bf16[96,2048]{1,0:T(8,128)(2,1)S(1)} collective-permute-done((bf16[96,2048]{1,0:T(8,128)(2,1)S(1)}, bf16[96,2048]{1,0:T(8,128)(2,1)S(1)}, u32[]{:S(2)}, u32[]{:S(2)}) %collective-permute-start.8) | collective-permute-done | bytes 393248 | tf_op jit(solution)/shard_map/ppermute | solution.py:21
  380.3 10.7 %collective-permute-done.9 = bf16[96,2048]{1,0:T(8,128)(2,1)S(1)} collective-permute-done((bf16[96,2048]{1,0:T(8,128)(2,1)S(1)}, bf16[96,2048]{1,0:T(8,128)(2,1)S(1)}, u32[]{:S(2)}, u32[]{:S(2)}) %collective-permute-start.9) | collective-permute-done | bytes 393248 | tf_op jit(solution)/shard_map/ppermute | solution.py:21
  391.8 10.5 %collective-permute-done.10 = bf16[96,2048]{1,0:T(8,128)(2,1)S(1)} collective-permute-done((bf16[96,2048]{1,0:T(8,128)(2,1)S(1)}, bf16[96,2048]{1,0:T(8,128)(2,1)S(1)}, u32[]{:S(2)}, u32[]{:S(2)}) %collective-permute-start.10) | collective-permute-done | bytes 393248 | tf_op jit(solution)/shard_map/ppermute | solution.py:21
  403.0 10.6 %collective-permute-done.11 = bf16[96,2048]{1,0:T(8,128)(2,1)S(1)} collective-permute-done((bf16[96,2048]{1,0:T(8,128)(2,1)S(1)}, bf16[96,2048]{1,0:T(8,128)(2,1)S(1)}, u32[]{:S(2)}, u32[]{:S(2)}) %collective-permute-start.11) | collective-permute-done | bytes 393248 | tf_op jit(solution)/shard_map/ppermute | solution.py:21
  414.3 12.2 %collective-permute-done.12 = bf16[96,2048]{1,0:T(8,128)(2,1)} collective-permute-done((bf16[96,2048]{1,0:T(8,128)(2,1)S(1)}, bf16[96,2048]{1,0:T(8,128)(2,1)}, u32[]{:S(2)}, u32[]{:S(2)}) %collective-permute-start.12) | collective-permute-done | bytes 393248 | tf_op jit(solution)/shard_map/ppermute | solution.py:21
  426.6 4.3 fusion.24
  431.3 2.0 copy.64
  433.3 1.9 copy.65
  435.2 2.1 collective-permute-done.13
  439.7 5.1 fusion.20
  444.9 13.3 %multiply_convert_fusion = bf16[768,2048]{1,0:T(8,128)(2,1)} fusion(bf16[2048,704]{1,0:T(8,128)(2,1)} %bitcast.66, f32[768,704]{0,1:T(8,128)} %fusion.20, bf16[2048,704]{1,0:T(8,128)(2,1)} %bitcast.64, s32[]{:T(128)S(6)} %select_n.13, bf16[768,2048]{1,0:T(8,128)(2,1)} %copy-done.15), kind=kOutput, calls=%fused_computation.4 | convolution fusion | flops 4442947584 | bytes 14221316 | tf_op jit(solution)/shard_map/dot_general | solution.py:68
  458.2 4.6 copy.69
  462.8 4.6 copy.70
  467.4 4.6 copy.71
  471.9 2.7 copy.66
  474.6 4.7 copy.67
  479.4 2.7 copy.68
  482.0 49.8 %reduce-scatter.5.cloned.1.call-done = bf16[96,2048]{1,0:T(8,128)(2,1)} async-done(((bf16[768,2048]{1,0:T(8,128)(2,1)}), bf16[96,2048]{1,0:T(8,128)(2,1)}) %reduce-scatter.5.cloned.1.call-update) | async-done | bytes 393232 | tf_op jit(solution)/shard_map/reduce_scatter | solution.py:66
  531.8 2.1 fusion.7
  (87 shorter events, 23.6 us)
Async XLA Ops:
  7.2 192.5 %all-gather.3.cloned.1.call-start = ((), (), s32[]{:S(2)}) async-start(), calls=%async_computation.6 | async-start | bytes 11796480 | tf_op jit(solution)/shard_map/all_gather | solution.py:39
  104.1 9.5 %copy-start = (bf16[96,2048]{1,0:T(8,128)(2,1)S(1)}, bf16[96,2048]{1,0:T(8,128)(2,1)}, u32[]{:S(2)}) copy-start(bf16[96,2048]{1,0:T(8,128)(2,1)} %param.11) | copy-start | bytes 1179652
  113.5 238.1 %reduce-scatter.3.cloned.1.call-start = ((), (), s32[]{:S(2)}) async-start(), calls=%async_computation.8 | async-start | bytes 3538944 | tf_op jit(solution)/shard_map/reduce_scatter | solution.py:66
  113.9 12.3 %collective-permute-start = (bf16[96,2048]{1,0:T(8,128)(2,1)S(1)}, bf16[96,2048]{1,0:T(8,128)(2,1)S(1)}, u32[]{:S(2)}, u32[]{:S(2)}) collective-permute-start(bf16[96,2048]{1,0:T(8,128)(2,1)S(1)} %fusion.3), channel_id=1, source_target_pairs={{0,2},{2,4},{4,6},{6,8},{8,10},{10,12},{12,14},{14,0},{1,3},{3,5},... | collective-permute-start | bytes 1179656 | tf_op jit(solution)/shard_map/ppermute | solution.py:21
  126.3 11.4 %collective-permute-start.1 = (bf16[96,2048]{1,0:T(8,128)(2,1)S(1)}, bf16[96,2048]{1,0:T(8,128)(2,1)S(1)}, u32[]{:S(2)}, u32[]{:S(2)}) collective-permute-start(bf16[96,2048]{1,0:T(8,128)(2,1)S(1)} %collective-permute-done), channel_id=1, source_target_pairs={{0,2},{2,4},{4,6},{6,8},{8,10},{10,12},{12,14},{14,0},{1,3},{3,5},... | collective-permute-start | bytes 1179656 | tf_op jit(solution)/shard_map/ppermute | solution.py:21
  137.7 10.6 %collective-permute-start.2 = (bf16[96,2048]{1,0:T(8,128)(2,1)S(1)}, bf16[96,2048]{1,0:T(8,128)(2,1)S(1)}, u32[]{:S(2)}, u32[]{:S(2)}) collective-permute-start(bf16[96,2048]{1,0:T(8,128)(2,1)S(1)} %collective-permute-done.1), channel_id=1, source_target_pairs={{0,2},{2,4},{4,6},{6,8},{8,10},{10,12},{12,14},{14,0},{1,3},{3,5},... | collective-permute-start | bytes 1179656 | tf_op jit(solution)/shard_map/ppermute | solution.py:21
  148.3 10.5 %collective-permute-start.3 = (bf16[96,2048]{1,0:T(8,128)(2,1)S(1)}, bf16[96,2048]{1,0:T(8,128)(2,1)S(1)}, u32[]{:S(2)}, u32[]{:S(2)}) collective-permute-start(bf16[96,2048]{1,0:T(8,128)(2,1)S(1)} %collective-permute-done.2), channel_id=1, source_target_pairs={{0,2},{2,4},{4,6},{6,8},{8,10},{10,12},{12,14},{14,0},{1,3},{3,5},... | collective-permute-start | bytes 1179656 | tf_op jit(solution)/shard_map/ppermute | solution.py:21
  158.7 11.5 %collective-permute-start.4 = (bf16[96,2048]{1,0:T(8,128)(2,1)S(1)}, bf16[96,2048]{1,0:T(8,128)(2,1)S(1)}, u32[]{:S(2)}, u32[]{:S(2)}) collective-permute-start(bf16[96,2048]{1,0:T(8,128)(2,1)S(1)} %collective-permute-done.3), channel_id=1, source_target_pairs={{0,2},{2,4},{4,6},{6,8},{8,10},{10,12},{12,14},{14,0},{1,3},{3,5},... | collective-permute-start | bytes 1179656 | tf_op jit(solution)/shard_map/ppermute | solution.py:21
  170.2 12.2 %collective-permute-start.5 = (bf16[96,2048]{1,0:T(8,128)(2,1)S(1)}, bf16[96,2048]{1,0:T(8,128)(2,1)S(1)}, u32[]{:S(2)}, u32[]{:S(2)}) collective-permute-start(bf16[96,2048]{1,0:T(8,128)(2,1)S(1)} %collective-permute-done.4), channel_id=1, source_target_pairs={{0,2},{2,4},{4,6},{6,8},{8,10},{10,12},{12,14},{14,0},{1,3},{3,5},... | collective-permute-start | bytes 1179656 | tf_op jit(solution)/shard_map/ppermute | solution.py:21
  182.4 10.9 %collective-permute-start.6 = (bf16[96,2048]{1,0:T(8,128)(2,1)S(1)}, bf16[96,2048]{1,0:T(8,128)(2,1)S(1)}, u32[]{:S(2)}, u32[]{:S(2)}) collective-permute-start(bf16[96,2048]{1,0:T(8,128)(2,1)S(1)} %collective-permute-done.5), channel_id=1, source_target_pairs={{0,2},{2,4},{4,6},{6,8},{8,10},{10,12},{12,14},{14,0},{1,3},{3,5},... | collective-permute-start | bytes 1179656 | tf_op jit(solution)/shard_map/ppermute | solution.py:21
  227.8 0.7 copy-start.16
  227.8 198.8 %all-gather.5.cloned.1.call-start = ((), (), s32[]{:S(2)}) async-start(), calls=%async_computation.7 | async-start | bytes 11796480 | tf_op jit(solution)/shard_map/all_gather | solution.py:39
  351.5 180.3 %reduce-scatter.5.cloned.1.call-start = ((), (), s32[]{:S(2)}) async-start(), calls=%async_computation.9 | async-start | bytes 3538944 | tf_op jit(solution)/shard_map/reduce_scatter | solution.py:66
  354.0 0.7 copy-start.3
  354.8 12.5 %collective-permute-start.7 = (bf16[96,2048]{1,0:T(8,128)(2,1)S(1)}, bf16[96,2048]{1,0:T(8,128)(2,1)S(1)}, u32[]{:S(2)}, u32[]{:S(2)}) collective-permute-start(bf16[96,2048]{1,0:T(8,128)(2,1)S(1)} %fusion.6), channel_id=1, source_target_pairs={{0,2},{2,4},{4,6},{6,8},{8,10},{10,12},{12,14},{14,0},{1,3},{3,5},... | collective-permute-start | bytes 1179656 | tf_op jit(solution)/shard_map/ppermute | solution.py:21
  367.2 0.7 copy-start.5
  368.0 11.6 %collective-permute-start.8 = (bf16[96,2048]{1,0:T(8,128)(2,1)S(1)}, bf16[96,2048]{1,0:T(8,128)(2,1)S(1)}, u32[]{:S(2)}, u32[]{:S(2)}) collective-permute-start(bf16[96,2048]{1,0:T(8,128)(2,1)S(1)} %collective-permute-done.7), channel_id=1, source_target_pairs={{0,2},{2,4},{4,6},{6,8},{8,10},{10,12},{12,14},{14,0},{1,3},{3,5},... | collective-permute-start | bytes 1179656 | tf_op jit(solution)/shard_map/ppermute | solution.py:21
  379.6 0.7 copy-start.7
  380.3 10.7 %collective-permute-start.9 = (bf16[96,2048]{1,0:T(8,128)(2,1)S(1)}, bf16[96,2048]{1,0:T(8,128)(2,1)S(1)}, u32[]{:S(2)}, u32[]{:S(2)}) collective-permute-start(bf16[96,2048]{1,0:T(8,128)(2,1)S(1)} %collective-permute-done.8), channel_id=1, source_target_pairs={{0,2},{2,4},{4,6},{6,8},{8,10},{10,12},{12,14},{14,0},{1,3},{3,5},... | collective-permute-start | bytes 1179656 | tf_op jit(solution)/shard_map/ppermute | solution.py:21
  391.0 0.7 copy-start.9
  391.8 10.5 %collective-permute-start.10 = (bf16[96,2048]{1,0:T(8,128)(2,1)S(1)}, bf16[96,2048]{1,0:T(8,128)(2,1)S(1)}, u32[]{:S(2)}, u32[]{:S(2)}) collective-permute-start(bf16[96,2048]{1,0:T(8,128)(2,1)S(1)} %collective-permute-done.9), channel_id=1, source_target_pairs={{0,2},{2,4},{4,6},{6,8},{8,10},{10,12},{12,14},{14,0},{1,3},{3,5},... | collective-permute-start | bytes 1179656 | tf_op jit(solution)/shard_map/ppermute | solution.py:21
  402.3 0.7 copy-start.11
  403.0 10.6 %collective-permute-start.11 = (bf16[96,2048]{1,0:T(8,128)(2,1)S(1)}, bf16[96,2048]{1,0:T(8,128)(2,1)S(1)}, u32[]{:S(2)}, u32[]{:S(2)}) collective-permute-start(bf16[96,2048]{1,0:T(8,128)(2,1)S(1)} %collective-permute-done.10), channel_id=1, source_target_pairs={{0,2},{2,4},{4,6},{6,8},{8,10},{10,12},{12,14},{14,0},{1,3},{3,5},... | collective-permute-start | bytes 1179656 | tf_op jit(solution)/shard_map/ppermute | solution.py:21
  413.6 0.7 copy-start.13
  414.3 12.3 %collective-permute-start.12 = (bf16[96,2048]{1,0:T(8,128)(2,1)S(1)}, bf16[96,2048]{1,0:T(8,128)(2,1)}, u32[]{:S(2)}, u32[]{:S(2)}) collective-permute-start(bf16[96,2048]{1,0:T(8,128)(2,1)S(1)} %collective-permute-done.11), channel_id=1, source_target_pairs={{0,2},{2,4},{4,6},{6,8},{8,10},{10,12},{12,14},{14,0},{1,3},{3,5},... | collective-permute-start | bytes 1179656 | tf_op jit(solution)/shard_map/ppermute | solution.py:21
  426.6 10.8 %collective-permute-start.13 = (bf16[96,2048]{1,0:T(8,128)(2,1)}, bf16[96,2048]{1,0:T(8,128)(2,1)}, u32[]{:S(2)}, u32[]{:S(2)}) collective-permute-start(bf16[96,2048]{1,0:T(8,128)(2,1)} %collective-permute-done.12), channel_id=1, source_target_pairs={{0,2},{2,4},{4,6},{6,8},{8,10},{10,12},{12,14},{14,0},{1,3},{3,5},... | collective-permute-start | bytes 1179656 | tf_op jit(solution)/shard_map/ppermute | solution.py:21
  431.2 8.5 %copy-start.2 = (bf16[1,2,8,2,64,704]{5,4,3,2,1,0:T(8,128)(2,1)}, bf16[1,2,8,2,64,704]{5,4,3,2,1,0:T(8,128)(2,1)S(1)}, u32[]{:S(2)}) copy-start(bf16[1,2,8,2,64,704]{5,4,3,2,1,0:T(8,128)(2,1)S(1)} %copy.63) | copy-start | bytes 8650756
  433.3 6.1 %copy-start.14 = (bf16[96,2048]{1,0:T(8,128)(2,1)S(1)}, bf16[96,2048]{1,0:T(8,128)(2,1)}, u32[]{:S(2)}) copy-start(bf16[96,2048]{1,0:T(8,128)(2,1)} %copy-done.13) | copy-start | bytes 1179652
  433.3 6.2 %copy-start.12 = (bf16[96,2048]{1,0:T(8,128)(2,1)S(1)}, bf16[96,2048]{1,0:T(8,128)(2,1)}, u32[]{:S(2)}) copy-start(bf16[96,2048]{1,0:T(8,128)(2,1)} %copy-done.11) | copy-start | bytes 1179652
  433.3 6.2 %copy-start.10 = (bf16[96,2048]{1,0:T(8,128)(2,1)S(1)}, bf16[96,2048]{1,0:T(8,128)(2,1)}, u32[]{:S(2)}) copy-start(bf16[96,2048]{1,0:T(8,128)(2,1)} %copy-done.9) | copy-start | bytes 1179652
  435.2 4.3 copy-start.8
  435.2 4.4 copy-start.6
  435.2 4.4 copy-start.4
  439.7 5.2 copy-start.15
  474.6 4.7 copy-start.1
Sparse Core Ops, SparseCore 0:
  113.7 62.6 all-gather.2
  227.9 91.3 reduce-scatter.2
  351.6 62.5 all-gather.4
  458.3 73.4 reduce-scatter.4
